TPU v7x, 32 devices: a whole 2x2x4 slice. The times are simulated.
32 devices in a mesh: sp: 4 (over y, x), tp: 8 (over z, core).
Axes of the slice: x: 2, y: 2, z: 4, core: 2. Of those that a mesh axis runs over, the one named last changes fastest.
Arguments:
- pool_input: bfloat16 [16384, 512], P('sp', 'tp'), may hold values from -6 to 6
- gate_pre: bfloat16 [16384, 1024], P(('sp', 'tp')), may hold values from -8 to 8
- resid: bfloat16 [16384, 1024], P(('sp', 'tp')), may hold values from -6 to 6
- docs: int32 [16384], P('sp'), may hold values from 0 to 3, never falling along the last dimension, each value on 1 to 8192 neighbouring positions
- w_up: bfloat16 [512, 1024], replicated, may hold values from -0.25 to 0.25
- w_out: bfloat16 [1024, 1024], replicated, may hold values from -0.1875 to 0.1875
- g_ffn: float32 [1024], replicated, may hold values from 0.1 to 1.9
- w_gate: bfloat16 [4, 1024, 1024], P('sp'), may hold values from -0.5 to 0.5
- w_lift: bfloat16 [4, 1024, 1024], P('sp'), may hold values from -0.5 to 0.5
- w_down: bfloat16 [4, 1024, 1024], P('sp'), may hold values from -0.0390625 to 0.0390625
- routes: int32 [16384, 2], P(('sp', 'tp')), may hold values from 0 to 3, all different within a row; in each aligned block of 512 rows (0 to 511, 512 to 1023, ...) at most 320 rows name the same one
- route_weight: float32 [16384, 2], P(('sp', 'tp')), may hold values from 0.2 to 1
Outputs:
- layer_out: bfloat16 [16384, 1024], P(('sp', 'tp'))
Inputs may be any that keep to these rules, and one draw needn't show every extreme that they name: `routes`: each row names 2 different experts; among the 512 rows of one device no expert is named more than 320 times. `docs`: document numbers never fall along the sequence.
All inputs are finite; a program needn't handle non-finite values.
Results may differ from a plain program's by a relative error of at most 0.0075.
Values may be sent and summed in bfloat16 or wider, within the bound.
A program may use at most 128 MiB of HBM per device.

v0:
```python
import jax
import jax.numpy as jnp
from jax import lax
from jax.sharding import PartitionSpec as P

POOL_W = 512
RIM = 15


def shifted_2(value, axis, steps):
    count = lax.axis_size(axis)
    leading, last = (max(0, -steps), min(count, count - steps))
    return lax.ppermute(value, axis, [(source, source + steps) for source in range(leading, last)])


def on_device(
    pool_input,
    gate_pre,
    resid,
    docs,
    w_up,
    w_out,
    g_ffn,
    w_gate,
    w_lift,
    w_down,
    routes,
    route_weight,
):
    tok_dev = pool_input.shape[0]
    channels = pool_input.shape[1]
    group_size = POOL_W // 4
    channel_ids = lax.axis_index("tp") * channels + lax.iota(jnp.int32, channels)
    window = jnp.power(2, channel_ids // group_size + 1)
    edge_rows = (pool_input[tok_dev - RIM :], docs[tok_dev - RIM :])
    before_rows, before_docs = shifted_2((edge_rows[0], edge_rows[1]), "sp", 1)
    first_dev = lax.axis_index("sp") == 0
    before_docs = jnp.where(first_dev, -1, before_docs)
    values = pool_input.astype(jnp.float32)
    padded = jnp.concatenate([before_rows.astype(jnp.float32), values], axis=0)
    doc_padded = jnp.concatenate([before_docs.astype(jnp.int32), docs], axis=0)
    running = jnp.zeros((tok_dev, channels), jnp.float32)
    counts = jnp.zeros((tok_dev, channels), jnp.float32)
    for offset in range(RIM + 1):
        shifted = padded[RIM - offset : RIM - offset + tok_dev]
        same_doc = (doc_padded[RIM - offset : RIM - offset + tok_dev] == docs).astype(jnp.float32)
        weight_mask = same_doc[:, None] * (offset < window).astype(jnp.float32)[None, :]
        running = running + weight_mask * shifted
        counts = counts + weight_mask
    pooled = (running / counts - values).astype(jnp.bfloat16)
    row_count = gate_pre.shape[0]
    tokens_pooled = lax.all_to_all(pooled, "tp", split_axis=0, concat_axis=1, tiled=True)
    lifted = jnp.dot(tokens_pooled, w_up, preferred_element_type=jnp.float32)
    gated_rows = (jax.nn.sigmoid(gate_pre.astype(jnp.float32)) * lifted).astype(jnp.bfloat16)
    mixed_rows = (
        resid.astype(jnp.float32) + jnp.dot(gated_rows, w_out, preferred_element_type=jnp.float32)
    ).astype(jnp.bfloat16)
    mixed_f = mixed_rows.astype(jnp.float32)
    normed = (
        mixed_f * lax.rsqrt(jnp.mean(mixed_f * mixed_f, axis=-1, keepdims=True) + 1e-06) * g_ffn
    ).astype(jnp.bfloat16)
    model_dim = normed.shape[1]
    top_count = routes.shape[1]
    local_experts = w_gate.shape[0]
    sp_count = lax.axis_size("sp")
    experts = sp_count * local_experts
    capacity = max(2, 5 * row_count * top_count // (4 * experts))
    flat_ids = routes.reshape(-1)
    onehot = (flat_ids[:, None] == lax.iota(jnp.int32, experts)[None, :]).astype(jnp.int32)
    slot_rank = jnp.sum((jnp.cumsum(onehot, axis=0) - onehot) * onehot, axis=1)
    slot_index = flat_ids * capacity + slot_rank
    source = normed[lax.iota(jnp.int32, row_count * top_count) // top_count]
    buffer = jnp.zeros((experts * capacity, model_dim), jnp.bfloat16).at[slot_index].set(source)
    buffer = buffer.reshape(sp_count, local_experts, capacity, model_dim)
    arrived = lax.all_to_all(buffer, "sp", split_axis=0, concat_axis=0, tiled=True)
    gate_act = jnp.minimum(
        jnp.einsum("sekd,edh->sekh", arrived, w_gate, preferred_element_type=jnp.float32), 7.0
    )
    lift = jnp.clip(
        jnp.einsum("sekd,edh->sekh", arrived, w_lift, preferred_element_type=jnp.float32), -7.0, 7.0
    )
    act = ((lift + 1.0) * gate_act * jax.nn.sigmoid(1.702 * gate_act)).astype(jnp.bfloat16)
    results = jnp.einsum("sekh,ehd->sekd", act, w_down, preferred_element_type=jnp.float32).astype(
        jnp.bfloat16
    )
    returned = lax.all_to_all(results, "sp", split_axis=0, concat_axis=0, tiled=True)
    picked = returned.reshape(experts * capacity, model_dim)[slot_index].astype(jnp.float32)
    picked = picked * route_weight.reshape(-1)[:, None]
    combined = jnp.sum(picked.reshape(row_count, top_count, model_dim), axis=1)
    return (mixed_f + combined).astype(jnp.bfloat16)


def solution(mesh):
    in_specs = (
        P("sp", "tp"),
        P(("sp", "tp"), None),
        P(("sp", "tp"), None),
        P("sp"),
        P(),
        P(),
        P(),
        P("sp", None, None),
        P("sp", None, None),
        P("sp", None, None),
        P(("sp", "tp"), None),
        P(("sp", "tp"), None),
    )
    out_specs = P(("sp", "tp"), None)
    return jax.shard_map(
        on_device, mesh=mesh, in_specs=in_specs, out_specs=out_specs, check_vma=False
    )
```

profile of v0, /device:TPU:0, one launch (start us, length us, event | category | flops | bytes accessed | tf_op | source)
XLA Modules:
  0.0 173.3 jit_solution(9526131367028028698)
XLA Ops:
  0.0 1.4 slice.102
  1.4 5.4 %collective-permute-start = (s32[15]{0:T(128)}, s32[15]{0:T(128)}, u32[]{:S(2)}, u32[]{:S(2)}) collective-permute-start(s32[15]{0:T(128)} %slice.102), channel_id=1, source_target_pairs={{0,8},{8,16},{16,24},{1,9},{9,17},{17,25},{2,10},{10,18},{18,26},{... | collective-permute-start | bytes 188 | tf_op jit(solution)/shard_map/ppermute | solution.py:13
  6.8 0.8 slice.104
  7.6 2.9 %collective-permute-start.1 = (bf16[15,64]{0,1:T(8,128)(2,1)S(1)}, bf16[15,64]{0,1:T(8,128)(2,1)S(1)}, u32[]{:S(2)}, u32[]{:S(2)}) collective-permute-start(bf16[15,64]{0,1:T(8,128)(2,1)S(1)} %slice.104), channel_id=1, source_target_pairs={{0,8},{8,16},{16,24},{1,9},{9,17},{17,25},{2,10},{10,18},{18,26},{... | collective-permute-start | bytes 5768 | tf_op jit(solution)/shard_map/ppermute | solution.py:13
  11.2 1.1 convert_element_type.219
  12.3 0.8 copy.25
  14.0 1.1 reduce-window.6
  15.5 5.8 %fusion.58 = bf16[4096,64]{0,1:T(8,128)(2,1)S(1)} fusion(f32[4096,64]{0,1:T(8,128)S(1)} %convert_element_type.219, f32[15,64]{0,1:T(8,128)S(1)} %convert_element_type.222, f32[64]{0:T(128)S(1)} %get-tuple-element.22, f32[4096]{0:T(1024)S(1)} %get-tuple-element.18, f32[64]{0:T(128)S(1)} %get-tuple-element.23, f32[4096]{0:T(1024)S(1)} %get-tuple-element.19, ...), kind=kLoop, calls=%fused_computation.114 | loop fusion | flops 20709376 | bytes 1826560 | tf_op jit(solution)/shard_map/convert_element_type | solution.py:50
  21.3 0.8 copy.33
  22.1 4.9 %all-to-all-start = ((bf16[8,512,64]{1,2,0:T(8,128)(2,1)}), bf16[8,512,64]{1,2,0:T(8,128)(2,1)S(1)}, u32[]{:S(2)}, u32[]{:S(2)}) async-start(bf16[8,512,64]{1,2,0:T(8,128)(2,1)} %bitcast.68), calls=%async_computation | async-start | bytes 1048576 | tf_op jit(solution)/shard_map/all_to_all | solution.py:52
  28.1 14.3 %all-to-all-done = bf16[8,512,64]{1,2,0:T(8,128)(2,1)S(1)} async-done(((bf16[8,512,64]{1,2,0:T(8,128)(2,1)}), bf16[8,512,64]{1,2,0:T(8,128)(2,1)S(1)}, u32[]{:S(2)}, u32[]{:S(2)}) %all-to-all-start) | async-done | bytes 524320 | tf_op jit(solution)/shard_map/all_to_all | solution.py:52
  43.1 4.6 %fusion.9 = (f32[512]{0:T(512)S(1)}, bf16[512,1024]{1,0:T(8,128)(2,1)S(1)}) fusion(bf16[1024,1024]{1,0:T(8,128)(2,1)} %param.17, bf16[512,1024]{1,0:T(8,128)(2,1)} %param.13, bf16[512,512]{0,1:T(8,128)(2,1)} %bitcast.72, bf16[512,1024]{1,0:T(8,128)(2,1)} %param.16, bf16[512,1024]{1,0:T(8,128)(2,1)} %param.14), kind=kOutput, calls=%fused_computation.28 | convolution fusion | flops 1616903680 | bytes 6817792 | tf_op jit(solution)/shard_map/dot_general | solution.py:56
  47.8 1.3 fusion.11
  49.1 15.9 %scatter_custom_fusion = bf16[1280,1024]{1,0:T(8,128)(2,1)} fusion(s32[1024]{0:T(1024)S(1)} %bitcast.73, bf16[512,1024]{1,0:T(8,128)(2,1)} %fusion.11, s32[1024]{0:T(1024)S(1)} %broadcast_clamp_fusion.1, bf16[]{:T(256)} %constant.106.clone.1), kind=kCustom, calls=%fused_computation.35 | custom fusion | bytes 2621952 | tf_op jit(solution)/shard_map/scatter | solution.py:73
  65.0 34.6 %all_to_all.29 = bf16[4,1,320,1024]{3,2,1,0:T(8,128)(2,1)S(1)} all-to-all(bf16[4,1,320,1024]{3,2,1,0:T(8,128)(2,1)} %bitcast.70), channel_id=1, replica_groups=mesh['sp'=4,'tp'=8] {'sp'}, dimensions={0} | all-to-all | bytes 5242880 | tf_op jit(solution)/shard_map/all_to_all | solution.py:75
  99.6 1.5 copy-done.1
  101.2 4.6 %fusion = f32[4,320,1024]{2,1,0:T(8,128)} fusion(bf16[4,1,320,1024]{3,2,1,0:T(8,128)(2,1)S(1)} %all_to_all.29, bf16[1,1024,1024]{2,1,0:T(8,128)(2,1)S(1)} %copy-done), kind=kOutput, calls=%fused_computation.22 | convolution fusion | flops 2684354560 | bytes 9961472 | tf_op jit(solution)/shard_map/sekd,edh->sekh/dot_general | solution.py:77
  105.7 10.5 %convert_bitcast_fusion = bf16[4,1,320,1024]{3,2,1,0:T(8,128)(2,1)} fusion(bf16[1,1024,1024]{2,1,0:T(8,128)(2,1)} %param.21, f32[4,320,1024]{2,1,0:T(8,128)} %fusion, bf16[4,1,320,1024]{3,2,1,0:T(8,128)(2,1)} %copy-done.1, bf16[1,1024,1024]{2,1,0:T(8,128)(2,1)} %param.20), kind=kOutput, calls=%fused_computation.26 | convolution fusion | flops 5383127040 | bytes 14680064 | tf_op jit(solution)/shard_map/sekh,ehd->sekd/dot_general | solution.py:83
  116.3 4.7 %all-to-all-start.2 = ((bf16[4,1,320,1024]{3,2,1,0:T(8,128)(2,1)}), bf16[4,1,320,1024]{3,2,1,0:T(8,128)(2,1)}, u32[]{:S(2)}, u32[]{:S(2)}) async-start(bf16[4,1,320,1024]{3,2,1,0:T(8,128)(2,1)} %convert_bitcast_fusion), calls=%async_computation.2 | async-start | bytes 5242880 | tf_op jit(solution)/shard_map/all_to_all | solution.py:86
  121.1 29.8 %all-to-all-done.2 = bf16[4,1,320,1024]{3,2,1,0:T(8,128)(2,1)} async-done(((bf16[4,1,320,1024]{3,2,1,0:T(8,128)(2,1)}), bf16[4,1,320,1024]{3,2,1,0:T(8,128)(2,1)}, u32[]{:S(2)}, u32[]{:S(2)}) %all-to-all-start.2) | async-done | bytes 2621472 | tf_op jit(solution)/shard_map/all_to_all | solution.py:86
  150.9 8.1 %gather_fusion = bf16[1024,1024]{1,0:T(8,128)(2,1)} fusion(bf16[1280,1024]{1,0:T(8,128)(2,1)} %bitcast.18, s32[1024]{0:T(1024)S(1)} %broadcast_clamp_fusion), kind=kCustom, calls=%fused_computation.1 | custom fusion | bytes 4198400 | tf_op jit(solution)/shard_map/gather | solution.py:87
  159.0 5.5 %reshape.280 = f32[512,2,1024]{2,1,0:T(2,128)} reshape(bf16[1024,1024]{1,0:T(8,128)(2,1)} %gather_fusion) | data formatting | bytes 6291456 | tf_op jit(solution)/shard_map/convert_element_type | solution.py:87
  164.5 7.5 %multiply_reduce_fusion = f32[512,1024]{1,0:T(8,128)S(1)} fusion(f32[512,2,1024]{2,1,0:T(2,128)} %reshape.280, f32[512,2]{1,0:T(8,128)S(1)} %copy.28), kind=kLoop, calls=%fused_computation.18 | loop fusion | flops 1572864 | bytes 6295552 | tf_op jit(solution)/shard_map/reduce_sum | solution.py:89
  172.0 1.4 fusion.12
  (41 shorter events, 3.8 us)
Async XLA Ops:
  0.0 101.2 %copy-start = (bf16[1,1024,1024]{2,1,0:T(8,128)(2,1)S(1)}, bf16[1,1024,1024]{2,1,0:T(8,128)(2,1)}, u32[]{:S(2)}) copy-start(bf16[1,1024,1024]{2,1,0:T(8,128)(2,1)} %param.19) | copy-start | bytes 6291460
  0.0 15.2 %copy-start.3 = (s32[4096]{0:T(1024)S(1)}, s32[4096]{0:T(1024)}, u32[]{:S(2)}) copy-start(s32[4096]{0:T(1024)} %param.15) | copy-start | bytes 49156
  1.4 13.8 %collective-permute-start = (s32[15]{0:T(128)}, s32[15]{0:T(128)}, u32[]{:S(2)}, u32[]{:S(2)}) collective-permute-start(s32[15]{0:T(128)} %slice.102), channel_id=1, source_target_pairs={{0,8},{8,16},{16,24},{1,9},{9,17},{17,25},{2,10},{10,18},{18,26},{... | collective-permute-start | bytes 188 | tf_op jit(solution)/shard_map/ppermute | solution.py:13
  7.6 7.8 %collective-permute-start.1 = (bf16[15,64]{0,1:T(8,128)(2,1)S(1)}, bf16[15,64]{0,1:T(8,128)(2,1)S(1)}, u32[]{:S(2)}, u32[]{:S(2)}) collective-permute-start(bf16[15,64]{0,1:T(8,128)(2,1)S(1)} %slice.104), channel_id=1, source_target_pairs={{0,8},{8,16},{16,24},{1,9},{9,17},{17,25},{2,10},{10,18},{18,26},{... | collective-permute-start | bytes 5768 | tf_op jit(solution)/shard_map/ppermute | solution.py:13
  22.1 20.2 %all-to-all-start = ((bf16[8,512,64]{1,2,0:T(8,128)(2,1)}), bf16[8,512,64]{1,2,0:T(8,128)(2,1)S(1)}, u32[]{:S(2)}, u32[]{:S(2)}) async-start(bf16[8,512,64]{1,2,0:T(8,128)(2,1)} %bitcast.68), calls=%async_computation | async-start | bytes 1048576 | tf_op jit(solution)/shard_map/all_to_all | solution.py:52
  42.3 0.8 copy-start.2
  43.1 4.6 %copy-start.4 = (f32[1024]{0:T(1024)S(1)}, f32[1024]{0:T(1024)}, u32[]{:S(2)}) copy-start(f32[1024]{0:T(1024)} %param.18) | copy-start | bytes 12292
  99.6 1.5 copy-start.1
  116.3 4.7 %copy-start.5 = (f32[512,2]{0,1:T(2,128)S(1)}, f32[512,2]{0,1:T(2,128)}, u32[]{:S(2)}) copy-start(f32[512,2]{0,1:T(2,128)} %param.23) | copy-start | bytes 12292
  116.3 34.6 %all-to-all-start.2 = ((bf16[4,1,320,1024]{3,2,1,0:T(8,128)(2,1)}), bf16[4,1,320,1024]{3,2,1,0:T(8,128)(2,1)}, u32[]{:S(2)}, u32[]{:S(2)}) async-start(bf16[4,1,320,1024]{3,2,1,0:T(8,128)(2,1)} %convert_bitcast_fusion), calls=%async_computation.2 | async-start | bytes 5242880 | tf_op jit(solution)/shard_map/all_to_all | solution.py:86
where the time goes:
time: 174 us; the launch traced here: 173 us
  waiting for transfers between devices  44.1 us (25%)
  local copies, waits for them, and re-layouts  36.7 us (21%)
  blocking collectives  34.6 us (20%)
  other arithmetic  20.2 us (12%)
  matrix products  19.7 us (11%)
  starting transfers between devices  17.8 us (10%)
    all_to_all x1, blocking collectives, on_device(): lax.all_to_all(buffer, 'sp', split_axis=0, concat_axis=0, tiled=True)  34.6 us
    all_to_all x1, waiting for transfers between devices, on_device(): lax.all_to_all(results, 'sp', split_axis=0, concat_axis=0, tiled=True)  29.8 us
    scatter x1, local copies, waits for them, and re-layouts, on_device(): jnp.zeros((experts * capacity, model_dim), jnp.bfloat16).at[slot_index]  15.9 us
    all_to_all x1, waiting for transfers between devices, on_device(): lax.all_to_all(pooled, 'tp', split_axis=0, concat_axis=1, tiled=True)  14.3 us
    dot_general x1, matrix products, on_device(): jnp.einsum('sekh,ehd->sekd', act, w_down, preferred_element_type=jnp.floa...  10.5 us
    ppermute x2, starting transfers between devices, shifted_2(): lax.ppermute(value, axis, [(source, source + steps) for source in range(l...  8.26 us
    gather x1, local copies, waits for them, and re-layouts, on_device(): returned.reshape(experts * capacity, model_dim)[slot_index]  8.12 us
    reduce_sum x1, other arithmetic, on_device(): combined = jnp.sum(picked.reshape(row_count, top_count, model_dim), axis=1)  7.51 us
  transfers between devices with their start and end apart: 4, of which 2 were waited for; matrix products, arithmetic and copies ran while one was open for 4% of the time, Pallas kernels for 0%

commit v1 on v0

v1 whole, which is shorter than its diff:
```python
import functools

import jax
import jax.numpy as jnp
from jax import lax
from jax.experimental import pallas as pl
from jax.experimental.pallas import tpu as pltpu
from jax.sharding import PartitionSpec as P

POOL_W = 512
RIM = 15
TILE = 256
MESH = pl.DeviceIdType.MESH


def shifted_2(value, axis, steps):
    count = lax.axis_size(axis)
    leading, last = (max(0, -steps), min(count, count - steps))
    return lax.ppermute(value, axis, [(source, source + steps) for source in range(leading, last)])


def partner(me, step, count):
    other, bit = 0, 1
    while bit < count:
        other = other + ((me // bit + step // bit) % 2) * bit
        bit *= 2
    return other


def tile_of(t):
    return pl.ds(pl.multiple_of(t * TILE, TILE), TILE)


def experts_kernel(
    count,
    mixed_ref,
    gain_ref,
    rank_rows_ref,
    rank_cols_ref,
    weight_ref,
    w_gate_hbm,
    w_lift_hbm,
    w_down_hbm,
    out_ref,
    normed,
    onehot,
    send,
    recv,
    result,
    back,
    total,
    act,
    w_gate,
    w_lift,
    w_down,
    weight_sems,
    go_sems,
    come_sems,
    ret_go_sems,
    ret_come_sems,
):
    rows, model_dim = mixed_ref.shape
    cap = send.shape[1]
    hidden = w_gate.shape[1]
    me = lax.axis_index("sp")
    loads = [
        pltpu.make_async_copy(src.at[0], dst, weight_sems.at[i])
        for i, (src, dst) in enumerate(
            ((w_gate_hbm, w_gate), (w_lift_hbm, w_lift), (w_down_hbm, w_down))
        )
    ]

    barrier = pltpu.get_barrier_semaphore()

    def greet(j, carry):
        pl.semaphore_signal(
            barrier, inc=1, device_id={"sp": partner(me, j, count)}, device_id_type=MESH
        )
        return carry

    lax.fori_loop(1, count, greet, 0)
    for load in loads:
        load.start()

    def norm(t, carry):
        block = pl.ds(pl.multiple_of(t * 64, 64), 64)
        x = mixed_ref[block, :].astype(jnp.float32)
        scale = lax.rsqrt(jnp.mean(x * x, axis=-1, keepdims=True) + 1e-06)
        normed[block, :] = (x * scale * gain_ref[...]).astype(jnp.bfloat16)
        return carry

    lax.fori_loop(0, rows // 64, norm, 0)

    def out_copy(j):
        return pltpu.make_async_remote_copy(
            src_ref=send.at[j],
            dst_ref=recv.at[j],
            send_sem=go_sems.at[j],
            recv_sem=come_sems.at[j],
            device_id={"sp": partner(me, j, count)},
            device_id_type=MESH,
        )

    def back_copy(j):
        return pltpu.make_async_remote_copy(
            src_ref=result.at[j],
            dst_ref=back.at[j],
            send_sem=ret_go_sems.at[j],
            recv_sem=ret_come_sems.at[j],
            device_id={"sp": partner(me, j, count)},
            device_id_type=MESH,
        )

    def pack(j, target):
        slot = lax.broadcasted_iota(jnp.int32, (cap, rows), 0)
        onehot[...] = (slot == rank_rows_ref[j]).astype(jnp.float32).astype(jnp.bfloat16)

        def piece(t, carry):
            cols = tile_of(t)
            target[j, :, cols] = jnp.dot(
                onehot[...], normed[:, cols], preferred_element_type=jnp.float32
            ).astype(jnp.bfloat16)
            return carry

        lax.fori_loop(0, model_dim // TILE, piece, 0)

    def ffn(j, source):
        def up(t, carry):
            cols = tile_of(t)
            x = source[j]
            gate = jnp.minimum(jnp.dot(x, w_gate[:, cols], preferred_element_type=jnp.float32), 7.0)
            lift = jnp.clip(
                jnp.dot(x, w_lift[:, cols], preferred_element_type=jnp.float32), -7.0, 7.0
            )
            act[:, cols] = ((lift + 1.0) * gate * jax.nn.sigmoid(1.702 * gate)).astype(jnp.bfloat16)
            return carry

        lax.fori_loop(0, hidden // TILE, up, 0)

        def down(t, carry):
            cols = tile_of(t)
            result[j, :, cols] = jnp.dot(
                act[...], w_down[:, cols], preferred_element_type=jnp.float32
            ).astype(jnp.bfloat16)
            return carry

        lax.fori_loop(0, model_dim // TILE, down, 0)

    def column(ref, j):
        lane = lax.broadcasted_iota(jnp.int32, ref.shape, 1)
        return jnp.sum(jnp.where(lane == j, ref[...], 0.0), axis=1, keepdims=True)

    def combine(j, source, store):
        rank = column(rank_cols_ref, j).astype(jnp.int32)
        weight = column(weight_ref, j)
        slot = lax.broadcasted_iota(jnp.int32, (rows, cap), 1)
        pick = (slot == rank).astype(jnp.float32).astype(jnp.bfloat16)

        def piece(t, carry):
            cols = tile_of(t)
            found = jnp.dot(pick, source[j, :, cols], preferred_element_type=jnp.float32)
            store(cols, weight * found)
            return carry

        lax.fori_loop(0, model_dim // TILE, piece, 0)

    def store_first(cols, term):
        total[:, cols] = mixed_ref[:, cols].astype(jnp.float32) + term

    def store_more(cols, term):
        total[:, cols] = total[:, cols] + term

    def store_last(cols, term):
        out_ref[:, cols] = (total[:, cols] + term).astype(jnp.bfloat16)

    pl.semaphore_wait(barrier, count - 1)

    def dispatch(j, carry):
        pack(j, send)
        out_copy(j).start()
        return carry

    lax.fori_loop(1, count, dispatch, 0)
    pack(0, send)
    for load in loads:
        load.wait()
    ffn(0, send)
    combine(0, result, store_first)

    def serve(j, carry):
        out_copy(j).wait_recv()
        ffn(j, recv)
        back_copy(j).start()
        return carry

    lax.fori_loop(1, count, serve, 0)

    def gather(j, carry):
        back_copy(j).wait_recv()
        combine(j, back, store_more)
        return carry

    lax.fori_loop(1, count - 1, gather, 0)
    back_copy(count - 1).wait_recv()
    combine(count - 1, back, store_last)

    def finish(j, carry):
        out_copy(j).wait_send()
        back_copy(j).wait_send()
        return carry

    lax.fori_loop(1, count, finish, 0)


def run_experts(mixed, gain, rank, weight, w_gate, w_lift, w_down, cap, count):
    rows, model_dim = mixed.shape
    hidden = w_gate.shape[2]
    vmem = pl.BlockSpec(memory_space=pltpu.VMEM)
    anywhere = pl.BlockSpec(memory_space=pl.ANY)
    slots = pltpu.VMEM((count, cap, model_dim), jnp.bfloat16)
    return pl.pallas_call(
        functools.partial(experts_kernel, count),
        out_shape=jax.ShapeDtypeStruct((rows, model_dim), jnp.bfloat16),
        in_specs=[vmem] * 5 + [anywhere] * 3,
        out_specs=vmem,
        scratch_shapes=[
            pltpu.VMEM((rows, model_dim), jnp.bfloat16),
            pltpu.VMEM((cap, rows), jnp.bfloat16),
            slots,
            slots,
            slots,
            slots,
            pltpu.VMEM((rows, model_dim), jnp.float32),
            pltpu.VMEM((cap, hidden), jnp.bfloat16),
            pltpu.VMEM(w_gate.shape[1:], jnp.bfloat16),
            pltpu.VMEM(w_lift.shape[1:], jnp.bfloat16),
            pltpu.VMEM(w_down.shape[1:], jnp.bfloat16),
            pltpu.SemaphoreType.DMA((3,)),
            pltpu.SemaphoreType.DMA((count,)),
            pltpu.SemaphoreType.DMA((count,)),
            pltpu.SemaphoreType.DMA((count,)),
            pltpu.SemaphoreType.DMA((count,)),
        ],
        compiler_params=pltpu.CompilerParams(
            collective_id=0, has_side_effects=True, vmem_limit_bytes=44 * 2**20
        ),
        cost_estimate=pl.CostEstimate(
            flops=6 * count * cap * model_dim * hidden,
            bytes_accessed=3 * model_dim * hidden * 2,
            transcendentals=count * cap * hidden,
        ),
    )(
        mixed,
        gain[None, :],
        rank.T[:, None, :],
        rank.astype(jnp.float32),
        weight,
        w_gate,
        w_lift,
        w_down,
    )


def on_device(
    pool_input,
    gate_pre,
    resid,
    docs,
    w_up,
    w_out,
    g_ffn,
    w_gate,
    w_lift,
    w_down,
    routes,
    route_weight,
):
    tok_dev = pool_input.shape[0]
    channels = pool_input.shape[1]
    group_size = POOL_W // 4
    channel_ids = lax.axis_index("tp") * channels + lax.iota(jnp.int32, channels)
    window = jnp.power(2, channel_ids // group_size + 1)
    edge = jnp.concatenate(
        [pool_input[tok_dev - RIM :], docs[tok_dev - RIM :, None].astype(jnp.bfloat16)], axis=1
    )
    before = shifted_2(edge, "sp", 1)
    before_rows = before[:, :channels]
    before_docs = before[:, channels].astype(jnp.int32)
    first_dev = lax.axis_index("sp") == 0
    before_docs = jnp.where(first_dev, -1, before_docs)
    values = pool_input.astype(jnp.float32)
    padded = jnp.concatenate([before_rows.astype(jnp.float32), values], axis=0)
    doc_padded = jnp.concatenate([before_docs.astype(jnp.int32), docs], axis=0)
    running = jnp.zeros((tok_dev, channels), jnp.float32)
    counts = jnp.zeros((tok_dev, channels), jnp.float32)
    for offset in range(RIM + 1):
        shifted = padded[RIM - offset : RIM - offset + tok_dev]
        same_doc = (doc_padded[RIM - offset : RIM - offset + tok_dev] == docs).astype(jnp.float32)
        weight_mask = same_doc[:, None] * (offset < window).astype(jnp.float32)[None, :]
        running = running + weight_mask * shifted
        counts = counts + weight_mask
    pooled = (running / counts - values).astype(jnp.bfloat16)
    tokens_pooled = lax.all_to_all(pooled, "tp", split_axis=0, concat_axis=1, tiled=True)
    lifted = jnp.dot(tokens_pooled, w_up, preferred_element_type=jnp.float32)
    gated_rows = (jax.nn.sigmoid(gate_pre.astype(jnp.float32)) * lifted).astype(jnp.bfloat16)
    mixed_rows = (
        resid.astype(jnp.float32) + jnp.dot(gated_rows, w_out, preferred_element_type=jnp.float32)
    ).astype(jnp.bfloat16)

    row_count, top_count = routes.shape
    count = lax.axis_size("sp")
    cap = max(2, 5 * row_count * top_count // (4 * count))
    cap = (cap + 15) // 16 * 16
    order = partner(lax.axis_index("sp"), lax.iota(jnp.int32, count), count)
    chosen = routes[:, :, None] == order[None, None, :]
    named = jnp.any(chosen, axis=1)
    rank = jnp.where(named, jnp.cumsum(named.astype(jnp.int32), axis=0) - 1, -1)
    weight = jnp.sum(jnp.where(chosen, route_weight[:, :, None], 0.0), axis=1)
    return run_experts(mixed_rows, g_ffn, rank, weight, w_gate, w_lift, w_down, cap, count)


def solution(mesh):
    in_specs = (
        P("sp", "tp"),
        P(("sp", "tp"), None),
        P(("sp", "tp"), None),
        P("sp"),
        P(),
        P(),
        P(),
        P("sp", None, None),
        P("sp", None, None),
        P("sp", None, None),
        P(("sp", "tp"), None),
        P(("sp", "tp"), None),
    )
    out_specs = P(("sp", "tp"), None)
    return jax.shard_map(
        on_device, mesh=mesh, in_specs=in_specs, out_specs=out_specs, check_vma=False
    )
```

time: 174 us -> 122 us (0.70)
  Pallas kernels: 0 us -> 64.7 us
  blocking collectives: 34.6 us -> 0 us
  waiting for transfers between devices: 44.1 us -> 13 us
  local copies, waits for them, and re-layouts: 36.7 us -> 10.5 us
  matrix products: 19.7 us -> 4.85 us
  starting transfers between devices: 17.8 us -> 9.75 us
  other arithmetic: 20.2 us -> 17.7 us
    pallas_call x0 -> x1, Pallas kernels: none -> 64.7 us  [run_experts(): pl.pallas_call(functools.partial(experts_kernel, count), out_shape=jax.Sh...]
    all_to_all x1 -> x0, blocking collectives: 34.6 us -> none  [on_device(): lax.all_to_all(buffer, 'sp', split_axis=0, concat_axis=0, tiled=True)]
    all_to_all x1 -> x0, waiting for transfers between devices: 29.8 us -> none  [on_device(): lax.all_to_all(results, 'sp', split_axis=0, concat_axis=0, tiled=True)]
    scatter x1 -> x0, local copies, waits for them, and re-layouts: 15.9 us -> none  [on_device(): jnp.zeros((experts * capacity, model_dim), jnp.bfloat16).at[slot_index]]
    dot_general x2 -> x0, matrix products: 15.1 us -> none  [the longest x1 10.5 us: on_device(): jnp.einsum('sekh,ehd->sekd', act, w_down, preferred_element_type=jnp.floa...]
    gather x1 -> x0, local copies, waits for them, and re-layouts: 8.12 us -> none  [on_device(): returned.reshape(experts * capacity, model_dim)[slot_index]]
    reduce_sum x2 -> x1, other arithmetic: 7.53 us -> 0.08 us  [on_device(): weight = jnp.sum(jnp.where(chosen, route_weight[:, :, None], 0.0), axis=1)]
    all_to_all x1 -> x0, starting transfers between devices: 4.67 us -> none  [on_device(): lax.all_to_all(results, 'sp', split_axis=0, concat_axis=0, tiled=True)]
  transfers between devices with their start and end apart: 4 -> 2, of which waited for: 2 -> 1; matrix products, arithmetic and copies ran while one was open for 4% -> 8% of each run, Pallas kernels for 0% -> 0%
where the time goes in v1:
time: 122 us; the launch traced here: 121 us
  Pallas kernels  64.7 us (53%)
  other arithmetic  17.7 us (15%)
  waiting for transfers between devices  13 us (11%)
  local copies, waits for them, and re-layouts  10.5 us (9%)
  starting transfers between devices  9.75 us (8%)
  matrix products  4.85 us (4%)
    pallas_call x1, Pallas kernels, run_experts(): pl.pallas_call(functools.partial(experts_kernel, count), out_shape=jax.Sh...  64.7 us
    all_to_all x1, waiting for transfers between devices, on_device(): lax.all_to_all(pooled, 'tp', split_axis=0, concat_axis=1, tiled=True)  13 us
    unnamed x24, local copies, waits for them, and re-layouts  7.08 us
    convert_element_type x1, other arithmetic, on_device(): pooled = (running / counts - values).astype(jnp.bfloat16)  6.12 us
    all_to_all x1, starting transfers between devices, on_device(): lax.all_to_all(pooled, 'tp', split_axis=0, concat_axis=1, tiled=True)  4.88 us
    ppermute x1, starting transfers between devices, shifted_2(): lax.ppermute(value, axis, [(source, source + steps) for source in range(l...  4.87 us
    dot_general x1, matrix products, on_device(): jnp.dot(gated_rows, w_out, preferred_element_type=jnp.float32)  4.85 us
    convert_element_type x8, other arithmetic, on_device(): (offset < window).astype(jnp.float32)[None, :]  4.81 us
  transfers between devices with their start and end apart: 2, of which 1 were waited for; matrix products, arithmetic and copies ran while one was open for 8% of the time, Pallas kernels for 0%

profile of v1, /device:TPU:0, one launch (start us, length us, event | category | flops | bytes accessed | tf_op | source)
XLA Modules:
  0.0 120.7 jit_solution(9614892008021624961)
XLA Ops:
  0.0 0.9 fusion.84
  1.0 0.8 slice.109
  2.0 4.9 %collective-permute-start = (bf16[15,65]{1,0:T(8,128)(2,1)S(1)}, bf16[15,65]{1,0:T(8,128)(2,1)S(1)}, u32[]{:S(2)}, u32[]{:S(2)}) collective-permute-start(bf16[15,65]{1,0:T(8,128)(2,1)S(1)} %pad_maximum_fusion.1), channel_id=1, source_target_pairs={{0,8},{8,16},{16,24},{1,9},{9,17},{17,25},{2,10},{10,18},{18,26},{... | collective-permute-start | bytes 5858 | tf_op jit(solution)/shard_map/ppermute | solution.py:19
  6.9 0.6 compare_convert_fusion.6
  7.5 0.6 compare_convert_fusion.12
  9.9 0.6 compare_convert_fusion.14
  10.5 0.6 compare_convert_fusion
  11.1 0.8 compare_reduce_fusion
  12.7 1.1 convert_element_type.194
  14.1 0.7 fusion.76
  14.8 0.8 fusion.77
  16.1 0.8 copy.49
  16.9 6.1 %fusion.32 = bf16[4096,64]{0,1:T(8,128)(2,1)S(1)} fusion(f32[4096,64]{0,1:T(8,128)S(1)} %convert_element_type.194, f32[15,64]{0,1:T(8,128)S(1)} %copy.49, f32[64]{0:T(128)} %get-tuple-element.20, f32[4096]{0:T(1024)} %get-tuple-element.18, f32[64]{0:T(128)} %get-tuple-element.21, f32[4096]{0:T(1024)} %get-tuple-element.19, f32[64]{0:T(128)} %get-tuple-element.22, ...), kind=kLoop, calls=%fused_computation.90 | loop fusion | flops 20709376 | bytes 1826560 | tf_op jit(solution)/shard_map/convert_element_type | solution.py:302
  23.1 0.8 copy.60
  23.9 4.9 %all-to-all-start = ((bf16[8,512,64]{1,2,0:T(8,128)(2,1)}), bf16[8,512,64]{1,2,0:T(8,128)(2,1)}, u32[]{:S(2)}, u32[]{:S(2)}) async-start(bf16[8,512,64]{1,2,0:T(8,128)(2,1)} %bitcast.24), calls=%async_computation | async-start | bytes 1048576 | tf_op jit(solution)/shard_map/all_to_all | solution.py:303
  29.2 1.2 %reduce-window.6 = s32[4,4,128]{2,1,0:T(4,128)S(1)} reduce-window(s32[4,4,128]{2,1,0:T(4,128)S(1)} %copy.52, s32[]{:T(128)} %constant.114.clone.1), window={size=1x1x128 pad=0_0x0_0x127_0}, to_apply=%region_1.2 | reduce-window | flops 260096 | bytes 16388 | tf_op jit(solution)/shard_map/reduce-window
  31.2 13.0 %all-to-all-done = bf16[8,512,64]{1,2,0:T(8,128)(2,1)} async-done(((bf16[8,512,64]{1,2,0:T(8,128)(2,1)}), bf16[8,512,64]{1,2,0:T(8,128)(2,1)}, u32[]{:S(2)}, u32[]{:S(2)}) %all-to-all-start) | async-done | bytes 524320 | tf_op jit(solution)/shard_map/all_to_all | solution.py:303
  44.2 4.8 %add_convert_fusion.mixed_ref = bf16[512,1024]{1,0:T(8,128)(2,1)} fusion(bf16[512,1024]{1,0:T(8,128)(2,1)} %param.14, bf16[1024,1024]{1,0:T(8,128)(2,1)S(1)} %copy-done, bf16[512,1024]{1,0:T(8,128)(2,1)} %param.13, bf16[512,512]{0,1:T(8,128)(2,1)} %bitcast.2, bf16[512,1024]{1,0:T(8,128)(2,1)} %param.16), kind=kOutput, calls=%fused_computation.14 | convolution fusion | flops 1615331328 | bytes 6815744 | tf_op jit(solution)/shard_map/dot_general | solution.py:307
  49.1 1.6 %copy-done.1 = bf16[1,1024,1024]{2,1,0:T(8,128)(2,1)S(1)} copy-done((bf16[1,1024,1024]{2,1,0:T(8,128)(2,1)S(1)}, bf16[1,1024,1024]{2,1,0:T(8,128)(2,1)}, u32[]{:S(2)}) %copy-start.1) | copy-done | bytes 2097176
  50.7 1.6 %copy-done.2 = bf16[1,1024,1024]{2,1,0:T(8,128)(2,1)S(1)} copy-done((bf16[1,1024,1024]{2,1,0:T(8,128)(2,1)S(1)}, bf16[1,1024,1024]{2,1,0:T(8,128)(2,1)}, u32[]{:S(2)}) %copy-start.2) | copy-done | bytes 2097176
  52.3 1.6 %copy-done.3 = bf16[1,1024,1024]{2,1,0:T(8,128)(2,1)S(1)} copy-done((bf16[1,1024,1024]{2,1,0:T(8,128)(2,1)S(1)}, bf16[1,1024,1024]{2,1,0:T(8,128)(2,1)}, u32[]{:S(2)}) %copy-start.3) | copy-done | bytes 2097176
  53.8 1.2 %copy-done.5 = bf16[512,1024]{1,0:T(8,128)(2,1)S(1)} copy-done((bf16[512,1024]{1,0:T(8,128)(2,1)S(1)}, bf16[512,1024]{1,0:T(8,128)(2,1)}, u32[]{:S(2)}) %copy-start.5) | copy-done | bytes 1048600
  55.1 64.7 %shard_map.118 = bf16[512,1024]{1,0:T(8,128)(2,1)S(1)} custom-call(bf16[512,1024]{1,0:T(8,128)(2,1)S(1)} %copy-done.5, f32[1,1024]{1,0:T(1,128)S(1)} %bitcast.26, s32[4,1,512]{2,1,0:T(1,128)S(1)} %copy.55.rank_rows_ref, f32[512,4]{1,0:T(8,128)S(1)} %fusion.33.rank_cols_ref, f32[512,4]{1,0:T(8,128)S(1)} %copy.56.weight_ref, ...), custom_call_target="tpu_custom_call" | custom-call | flops 8053063680 | bytes 6291456 | tf_op jit(solution)/shard_map/pallas_call | solution.py:221
  119.8 1.0 copy.62
  (41 shorter events, 4.8 us)
Async XLA Ops:
  0.0 44.2 %copy-start = (bf16[1024,1024]{1,0:T(8,128)(2,1)S(1)}, bf16[1024,1024]{1,0:T(8,128)(2,1)}, u32[]{:S(2)}) copy-start(bf16[1024,1024]{1,0:T(8,128)(2,1)} %param.17) | copy-start | bytes 6291460
  0.0 14.0 %copy-start.6 = (s32[4096]{0:T(1024)S(1)}, s32[4096]{0:T(1024)}, u32[]{:S(2)}) copy-start(s32[4096]{0:T(1024)} %param.15) | copy-start | bytes 49156
  2.0 11.8 %collective-permute-start = (bf16[15,65]{1,0:T(8,128)(2,1)S(1)}, bf16[15,65]{1,0:T(8,128)(2,1)S(1)}, u32[]{:S(2)}, u32[]{:S(2)}) collective-permute-start(bf16[15,65]{1,0:T(8,128)(2,1)S(1)} %pad_maximum_fusion.1), channel_id=1, source_target_pairs={{0,8},{8,16},{16,24},{1,9},{9,17},{17,25},{2,10},{10,18},{18,26},{... | collective-permute-start | bytes 5858 | tf_op jit(solution)/shard_map/ppermute | solution.py:19
  11.1 2.7 %copy-start.9 = (s32[4]{0:T(128)}, s32[4]{0:T(128)S(1)}, u32[]{:S(2)}) copy-start(s32[4]{0:T(128)S(1)} %fusion.79) | copy-start | bytes 52
  23.0 5.8 %copy-start.7 = (s32[512,2]{0,1:T(2,128)S(1)}, s32[512,2]{0,1:T(2,128)}, u32[]{:S(2)}) copy-start(s32[512,2]{0,1:T(2,128)} %param.22) | copy-start | bytes 12292
  23.0 5.7 %copy-start.8 = (f32[512,2]{0,1:T(2,128)S(1)}, f32[512,2]{0,1:T(2,128)}, u32[]{:S(2)}) copy-start(f32[512,2]{0,1:T(2,128)} %param.23) | copy-start | bytes 12292
  23.0 5.7 %copy-start.10 = (s32[4]{0:T(128)S(1)}, s32[4]{0:T(128)}, u32[]{:S(2)}) copy-start(s32[4]{0:T(128)} %copy-done.9) | copy-start | bytes 52
  23.9 20.3 %all-to-all-start = ((bf16[8,512,64]{1,2,0:T(8,128)(2,1)}), bf16[8,512,64]{1,2,0:T(8,128)(2,1)}, u32[]{:S(2)}, u32[]{:S(2)}) async-start(bf16[8,512,64]{1,2,0:T(8,128)(2,1)} %bitcast.24), calls=%async_computation | async-start | bytes 1048576 | tf_op jit(solution)/shard_map/all_to_all | solution.py:303
  44.2 4.9 %copy-start.4 = (f32[1024]{0:T(1024)S(1)}, f32[1024]{0:T(1024)}, u32[]{:S(2)}) copy-start(f32[1024]{0:T(1024)} %param.18) | copy-start | bytes 12292
  49.1 1.6 %copy-start.1 = (bf16[1,1024,1024]{2,1,0:T(8,128)(2,1)S(1)}, bf16[1,1024,1024]{2,1,0:T(8,128)(2,1)}, u32[]{:S(2)}) copy-start(bf16[1,1024,1024]{2,1,0:T(8,128)(2,1)} %w_gate_hbm.1) | copy-start | bytes 6291460
  50.7 1.6 %copy-start.2 = (bf16[1,1024,1024]{2,1,0:T(8,128)(2,1)S(1)}, bf16[1,1024,1024]{2,1,0:T(8,128)(2,1)}, u32[]{:S(2)}) copy-start(bf16[1,1024,1024]{2,1,0:T(8,128)(2,1)} %w_lift_hbm.1) | copy-start | bytes 6291460
  52.2 1.6 %copy-start.3 = (bf16[1,1024,1024]{2,1,0:T(8,128)(2,1)S(1)}, bf16[1,1024,1024]{2,1,0:T(8,128)(2,1)}, u32[]{:S(2)}) copy-start(bf16[1,1024,1024]{2,1,0:T(8,128)(2,1)} %w_down_hbm.1) | copy-start | bytes 6291460
  53.8 1.2 %copy-start.5 = (bf16[512,1024]{1,0:T(8,128)(2,1)S(1)}, bf16[512,1024]{1,0:T(8,128)(2,1)}, u32[]{:S(2)}) copy-start(bf16[512,1024]{1,0:T(8,128)(2,1)} %add_convert_fusion.mixed_ref) | copy-start | bytes 3145732

commit v2 on v1

--- a/solution.py
+++ b/solution.py
@@ -242,7 +242,7 @@
             pltpu.SemaphoreType.DMA((count,)),
         ],
         compiler_params=pltpu.CompilerParams(
-            collective_id=0, has_side_effects=True, vmem_limit_bytes=44 * 2**20
+            collective_id=0, has_side_effects=True, vmem_limit_bytes=60 * 2**20
         ),
         cost_estimate=pl.CostEstimate(
             flops=6 * count * cap * model_dim * hidden,
@@ -291,14 +291,16 @@
     values = pool_input.astype(jnp.float32)
     padded = jnp.concatenate([before_rows.astype(jnp.float32), values], axis=0)
     doc_padded = jnp.concatenate([before_docs.astype(jnp.int32), docs], axis=0)
-    running = jnp.zeros((tok_dev, channels), jnp.float32)
-    counts = jnp.zeros((tok_dev, channels), jnp.float32)
-    for offset in range(RIM + 1):
+    earlier = sum(
+        (doc_padded[RIM - offset : RIM - offset + tok_dev] == docs).astype(jnp.int32)
+        for offset in range(1, RIM + 1)
+    )
+    reach = jnp.minimum(earlier[:, None] + 1, window[None, :])
+    running = values
+    for offset in range(1, RIM + 1):
         shifted = padded[RIM - offset : RIM - offset + tok_dev]
-        same_doc = (doc_padded[RIM - offset : RIM - offset + tok_dev] == docs).astype(jnp.float32)
-        weight_mask = same_doc[:, None] * (offset < window).astype(jnp.float32)[None, :]
-        running = running + weight_mask * shifted
-        counts = counts + weight_mask
+        running = running + jnp.where(offset < reach, shifted, 0.0)
+    counts = reach.astype(jnp.float32)
     pooled = (running / counts - values).astype(jnp.bfloat16)
     tokens_pooled = lax.all_to_all(pooled, "tp", split_axis=0, concat_axis=1, tiled=True)
     lifted = jnp.dot(tokens_pooled, w_up, preferred_element_type=jnp.float32)

time: 122 us -> 110 us (0.902)
  other arithmetic: 17.7 us -> 9.98 us
  local copies, waits for them, and re-layouts: 10.5 us -> 6.46 us
  Pallas kernels: 64.7 us -> 67.4 us
  waiting for transfers between devices: 13 us -> 10.9 us
    convert_element_type x10 -> x0, other arithmetic: 6.27 us -> none  [the longest x8 4.81 us: on_device(): (offset < window).astype(jnp.float32)[None, :]]
    unnamed x24 -> x10, local copies, waits for them, and re-layouts: 7.08 us -> 2.36 us
    pallas_call x1, Pallas kernels: 64.7 us -> 67.4 us  [run_experts(): pl.pallas_call(functools.partial(experts_kernel, count), out_shape=jax.Sh...]
    all_to_all x1, waiting for transfers between devices: 13 us -> 10.9 us  [on_device(): lax.all_to_all(pooled, 'tp', split_axis=0, concat_axis=1, tiled=True)]
    convert_element_type x1, other arithmetic: 6.12 us -> 4.35 us  [on_device(): pooled = (running / counts - values).astype(jnp.bfloat16)]
  transfers between devices with their start and end apart: 2 -> 2, of which waited for: 1 -> 1; matrix products, arithmetic and copies ran while one was open for 8% -> 6% of each run, Pallas kernels for 0% -> 0%
where the time goes in v2:
time: 110 us; the launch traced here: 109 us
  Pallas kernels  67.4 us (61%)
  waiting for transfers between devices  10.9 us (10%)
  other arithmetic  9.98 us (9%)
  starting transfers between devices  9.75 us (9%)
  local copies, waits for them, and re-layouts  6.46 us (6%)
  matrix products  4.68 us (4%)
    pallas_call x1, Pallas kernels, run_experts(): pl.pallas_call(functools.partial(experts_kernel, count), out_shape=jax.Sh...  67.4 us
    all_to_all x1, waiting for transfers between devices, on_device(): lax.all_to_all(pooled, 'tp', split_axis=0, concat_axis=1, tiled=True)  10.9 us
    all_to_all x1, starting transfers between devices, on_device(): lax.all_to_all(pooled, 'tp', split_axis=0, concat_axis=1, tiled=True)  4.88 us
    ppermute x1, starting transfers between devices, shifted_2(): lax.ppermute(value, axis, [(source, source + steps) for source in range(l...  4.87 us
    dot_general x1, matrix products, on_device(): jnp.dot(gated_rows, w_out, preferred_element_type=jnp.float32)  4.68 us
    convert_element_type x1, other arithmetic, on_device(): pooled = (running / counts - values).astype(jnp.bfloat16)  4.35 us
    unnamed x10, local copies, waits for them, and re-layouts  2.36 us
  transfers between devices with their start and end apart: 2, of which 1 were waited for; matrix products, arithmetic and copies ran while one was open for 6% of the time, Pallas kernels for 0%

profile of v2, /device:TPU:0, one launch (start us, length us, event | category | flops | bytes accessed | tf_op | source)
XLA Modules:
  0.0 109.3 jit_solution(14522199825797948476)
XLA Ops:
  0.0 0.9 fusion.84
  0.9 0.1 copy.48
  1.0 0.8 slice.109
  2.0 4.9 %collective-permute-start = (bf16[15,65]{1,0:T(8,128)(2,1)S(1)}, bf16[15,65]{1,0:T(8,128)(2,1)S(1)}, u32[]{:S(2)}, u32[]{:S(2)}) collective-permute-start(bf16[15,65]{1,0:T(8,128)(2,1)S(1)} %pad_maximum_fusion.1), channel_id=1, source_target_pairs={{0,8},{8,16},{16,24},{1,9},{9,17},{17,25},{2,10},{10,18},{18,26},{... | collective-permute-start | bytes 5858 | tf_op jit(solution)/shard_map/ppermute | solution.py:19
  6.9 0.8 compare_reduce_fusion
  7.7 0.2 copy.51
  7.9 1.1 %convert_element_type.84 = f32[4096,64]{0,1:T(8,128)S(1)} convert(bf16[4096,64]{0,1:T(8,128)(2,1)} %param.12) | non-fusion elementwise | flops 262144 | bytes 1572864 | tf_op jit(solution)/shard_map/convert_element_type | solution.py:291
  9.1 0.2 select_reduce_fusion
  9.3 0.1 add_add_fusion
  9.5 4.4 %fusion.47 = bf16[4096,64]{0,1:T(8,128)(2,1)S(1)} fusion(f32[4096,64]{0,1:T(8,128)S(1)} %convert_element_type.84, f32[15,64]{0,1:T(8,128)S(1)} %copy.49, s32[64]{0:T(128)S(1)} %compare_select_fusion.10, s32[4096]{0:T(1024)S(1)} %add_add_fusion), kind=kLoop, calls=%fused_computation.91 | loop fusion | flops 17039360 | bytes 1593344 | tf_op jit(solution)/shard_map/convert_element_type | solution.py:304
  13.9 0.8 copy.60
  14.8 4.9 %all-to-all-start = ((bf16[8,512,64]{1,2,0:T(8,128)(2,1)}), bf16[8,512,64]{1,2,0:T(8,128)(2,1)S(1)}, u32[]{:S(2)}, u32[]{:S(2)}) async-start(bf16[8,512,64]{1,2,0:T(8,128)(2,1)} %bitcast.24), calls=%async_computation | async-start | bytes 1048576 | tf_op jit(solution)/shard_map/all_to_all | solution.py:305
  19.7 0.9 copy.56.weight_ref
  20.6 0.1 copy.52
  20.7 1.2 %reduce-window.6 = s32[4,4,128]{2,1,0:T(4,128)S(1)} reduce-window(s32[4,4,128]{2,1,0:T(4,128)S(1)} %copy.52, s32[]{:T(128)} %constant.116.clone.1), window={size=1x1x128 pad=0_0x0_0x127_0}, to_apply=%region_1.2 | reduce-window | flops 260096 | bytes 16388 | tf_op jit(solution)/shard_map/reduce-window
  21.9 0.2 slice_reduce_fusion
  22.2 0.2 reduce-window.9
  22.4 0.2 copy.53
  22.6 0.7 copy.55.rank_rows_ref
  23.3 0.8 fusion.48.rank_cols_ref
  24.1 10.9 %all-to-all-done = bf16[8,512,64]{1,2,0:T(8,128)(2,1)S(1)} async-done(((bf16[8,512,64]{1,2,0:T(8,128)(2,1)}), bf16[8,512,64]{1,2,0:T(8,128)(2,1)S(1)}, u32[]{:S(2)}, u32[]{:S(2)}) %all-to-all-start) | async-done | bytes 524320 | tf_op jit(solution)/shard_map/all_to_all | solution.py:305
  35.0 4.7 %add_convert_fusion.mixed_ref = bf16[512,1024]{1,0:T(8,128)(2,1)} fusion(bf16[512,1024]{1,0:T(8,128)(2,1)} %param.14, bf16[1024,1024]{1,0:T(8,128)(2,1)S(1)} %copy-done, bf16[512,1024]{1,0:T(8,128)(2,1)} %param.13, bf16[512,512]{0,1:T(8,128)(2,1)S(1)} %bitcast.29, bf16[512,1024]{1,0:T(8,128)(2,1)} %param.16), kind=kOutput, calls=%fused_computation.30 | convolution fusion | flops 1615331328 | bytes 6815744 | tf_op jit(solution)/shard_map/dot_general | solution.py:309
  39.6 67.4 %shard_map.118 = bf16[512,1024]{1,0:T(8,128)(2,1)} custom-call(bf16[512,1024]{1,0:T(8,128)(2,1)} %add_convert_fusion.mixed_ref, f32[1,1024]{1,0:T(1,128)} %bitcast.31, s32[4,1,512]{2,1,0:T(1,128)} %copy.55.rank_rows_ref, f32[512,4]{1,0:T(8,128)} %fusion.48.rank_cols_ref, f32[512,4]{1,0:T(8,128)} %copy.56.weight_ref, bf16[1,1024,1024]{2,1,0:T(8,128)(2,1)} %w_gate_hbm.1, ...), custom_call_target="tpu_custom_call" | custom-call | flops 8053063680 | bytes 6291456 | tf_op jit(solution)/shard_map/pallas_call | solution.py:221
  107.0 2.3 %copy.62 = bf16[512,1024]{1,0:T(8,128)(2,1)} copy(bf16[512,1024]{1,0:T(8,128)(2,1)} %shard_map.118) | data formatting | bytes 2097152
  (19 shorter events, 0.5 us)
Async XLA Ops:
  0.0 35.0 %copy-start = (bf16[1024,1024]{1,0:T(8,128)(2,1)S(1)}, bf16[1024,1024]{1,0:T(8,128)(2,1)}, u32[]{:S(2)}) copy-start(bf16[1024,1024]{1,0:T(8,128)(2,1)} %param.17) | copy-start | bytes 6291460
  0.0 9.3 %copy-start.1 = (s32[4096]{0:T(1024)S(1)}, s32[4096]{0:T(1024)}, u32[]{:S(2)}) copy-start(s32[4096]{0:T(1024)} %param.15) | copy-start | bytes 49156
  2.0 7.1 %collective-permute-start = (bf16[15,65]{1,0:T(8,128)(2,1)S(1)}, bf16[15,65]{1,0:T(8,128)(2,1)S(1)}, u32[]{:S(2)}, u32[]{:S(2)}) collective-permute-start(bf16[15,65]{1,0:T(8,128)(2,1)S(1)} %pad_maximum_fusion.1), channel_id=1, source_target_pairs={{0,8},{8,16},{16,24},{1,9},{9,17},{17,25},{2,10},{10,18},{18,26},{... | collective-permute-start | bytes 5858 | tf_op jit(solution)/shard_map/ppermute | solution.py:19
  9.1 10.6 %copy-start.2 = (s32[512,2]{0,1:T(2,128)S(1)}, s32[512,2]{0,1:T(2,128)}, u32[]{:S(2)}) copy-start(s32[512,2]{0,1:T(2,128)} %param.22) | copy-start | bytes 12292
  9.1 10.6 %copy-start.3 = (f32[512,2]{0,1:T(2,128)S(1)}, f32[512,2]{0,1:T(2,128)}, u32[]{:S(2)}) copy-start(f32[512,2]{0,1:T(2,128)} %param.23) | copy-start | bytes 12292
  14.8 20.2 %all-to-all-start = ((bf16[8,512,64]{1,2,0:T(8,128)(2,1)}), bf16[8,512,64]{1,2,0:T(8,128)(2,1)S(1)}, u32[]{:S(2)}, u32[]{:S(2)}) async-start(bf16[8,512,64]{1,2,0:T(8,128)(2,1)} %bitcast.24), calls=%async_computation | async-start | bytes 1048576 | tf_op jit(solution)/shard_map/all_to_all | solution.py:305
